TPU v7x, 1024 devices: a whole 4x4x32 slice. The times are simulated.
1024 devices in a mesh: ep: 64 (over z, core), tp: 16 (over y, x).
Axes of the slice: x: 4, y: 4, z: 32, core: 2. Of those that a mesh axis runs over, the one named last changes fastest.
Arguments:
- tokens: bfloat16 [8192, 2048], P('ep', 'tp'), may hold values from -6 to 6
- routing: int32 [8192, 2], P('ep'), may hold values from 0 to 31, all different within a row; in each aligned block of 128 rows (0 to 127, 128 to 255, ...) at most 10 rows name the same one
- mixing: float32 [8192, 2], P('ep'), may hold values from 0.1 to 0.9
- gate_matrix: bfloat16 [64, 2048, 2048], P('ep', None, 'tp'), may hold values from -0.125 to 0.125
- up_matrix: bfloat16 [64, 2048, 2048], P('ep', None, 'tp'), may hold values from -0.125 to 0.125
- down_matrix: bfloat16 [64, 2048, 2048], P('ep', 'tp'), may hold values from -0.09375 to 0.09375
- upstream: bfloat16 [8192, 2048], P('ep', 'tp'), may hold values from -6 to 6
Outputs:
- token_gradient: bfloat16 [8192, 2048], P('ep', 'tp')
- mixing_gradient: float32 [8192, 2], P('ep')
- gate_gradient: bfloat16 [64, 2048, 2048], P('ep', None, 'tp')
- up_gradient: bfloat16 [64, 2048, 2048], P('ep', None, 'tp')
- down_gradient: bfloat16 [64, 2048, 2048], P('ep', 'tp')
- input_norms: float32 [64, 2, 2048], P('ep')
- down_norms: float32 [64, 2048], P('ep', 'tp')
Inputs may be any that keep to these rules, and one draw needn't show every extreme that they name: `routing`: A token's 2 experts differ. In each aligned block of 128 rows (the rows of one index of ep) no expert is named by more than 10 rows, and in every draw some expert is named by exactly 10 rows of some block.
All inputs are finite; a program needn't handle non-finite values.
Results may differ from a plain program's by a relative error of at most 0.0064.
Values may be sent and summed in bfloat16 or wider, within the bound.
A program may use at most 64 MiB of HBM per device.

v0:
```python
import jax
import jax.numpy as jnp
from jax import lax
from jax.sharding import PartitionSpec as P


def side_by_side(arrays, axis, split_dim, concat_dim, along):
    widths = [a.shape[along] for a in arrays]
    both = jnp.concatenate(arrays, axis=along)
    result = lax.all_to_all(both, axis, split_axis=split_dim, concat_axis=concat_dim, tiled=True)
    return tuple(jnp.split(result, [sum(widths[:k]) for k in range(1, len(widths))], axis=along))


def sent_together(arrays, axis, dim, along):
    ends, at = ([], 0)
    for a in arrays[:-1]:
        at += a.shape[along]
        ends.append(at)
    both = jnp.concatenate(arrays, axis=along)
    return tuple(jnp.split(lax.all_gather(both, axis, axis=dim, tiled=True), ends, axis=along))


def swapped(block, axis, distance):
    count = lax.axis_size(axis)
    route = []
    for low in range(count):
        high = low | 1 << distance
        if high != low and high < count:
            route += [(low, high), (high, low)]
    return lax.ppermute(block, axis, route)


def copy_for_each(value, axis):
    count = lax.axis_size(axis)
    return lax.all_to_all(
        jnp.broadcast_to(value[None], (count, *value.shape)), axis, 0, 0, tiled=True
    )


def of_everyone(value, axis):
    everything = copy_for_each(value, axis)
    return jnp.sum(everything, axis=0)


def in_one(arrays, axis):
    ends = [0]
    for a in arrays:
        ends.append(ends[-1] + a.size)
    running = of_everyone(jnp.concatenate([a.ravel() for a in arrays]), axis)
    return tuple((running[b:e].reshape(a.shape) for a, b, e in zip(arrays, ends, ends[1:])))


def sent_together_2(arrays, axis, split_dim, concat_dim, along):
    columns = [a.reshape(*a.shape[:along], -1) for a in arrays]
    both = jnp.concatenate(columns, axis=along)
    result, at, gathered = (
        lax.all_to_all(both, axis, split_axis=split_dim, concat_axis=concat_dim, tiled=True),
        0,
        [],
    )
    for a, column in zip(arrays, columns):
        piece = result[..., at : at + column.shape[along]]
        gathered.append(piece.reshape(*piece.shape[:along], *a.shape[along:]))
        at += column.shape[along]
    return tuple(gathered)


def slot_targets(route_block, experts, capacity):
    flat_routes = route_block.reshape(-1)
    choose = (flat_routes[:, None] == jnp.arange(experts, dtype=jnp.int32)[None, :]).astype(
        jnp.int32
    )
    earlier = jnp.cumsum(choose, axis=0) - choose
    return flat_routes * capacity + jnp.sum(earlier * choose, axis=1)


def place_rows(target, values, slot_count):
    matches = (target[:, None] == jnp.arange(slot_count, dtype=jnp.int32)[None, :]).astype(
        values.dtype
    )
    placed = lax.dot_general(
        matches, values, (((0,), (0,)), ((), ())), preferred_element_type=jnp.float32
    )
    return placed.astype(jnp.bfloat16)


def on_device(tokens, routing, mixing, gate_matrix, up_matrix, down_matrix, upstream):
    experts = lax.axis_size("ep") // 2
    tp_count = lax.axis_size("tp")
    tok_rows, part_width = tokens.shape
    top_count = routing.shape[1]
    capacity = 5 * top_count * tok_rows // (4 * experts)
    target = slot_targets(routing, experts, capacity)
    scaled = (mixing[:, :, None] * upstream[:, None, :].astype(jnp.float32)).astype(jnp.bfloat16)
    placed_tokens = place_rows(target, jnp.repeat(tokens, top_count, axis=0), experts * capacity)
    placed_grads = place_rows(
        target, scaled.reshape(tok_rows * top_count, part_width), experts * capacity
    )
    half_shape = (2 * experts, capacity // 2, part_width)
    arrived = side_by_side(
        (placed_tokens.reshape(half_shape), placed_grads.reshape(half_shape)), "ep", 0, 0, 1
    )
    token_rows, grad_rows = sent_together((arrived[0][None], arrived[1][None]), "tp", 0, 1)
    other_tokens, other_grads = swapped((token_rows, grad_rows), "ep", 0)
    lower_half = lax.axis_index("ep") % 2 == 0
    token_rows = jnp.where(
        lower_half,
        jnp.concatenate([token_rows, other_tokens], axis=2),
        jnp.concatenate([other_tokens, token_rows], axis=2),
    )
    grad_rows = jnp.where(
        lower_half,
        jnp.concatenate([grad_rows, other_grads], axis=2),
        jnp.concatenate([other_grads, grad_rows], axis=2),
    )
    sources = token_rows.shape[1]
    row_count = sources * capacity
    token_blocks = token_rows.reshape(tp_count, row_count, part_width)
    grad_blocks = grad_rows.reshape(tp_count, row_count, part_width)
    hidden_dev = gate_matrix.shape[2]
    full_width = tp_count * part_width
    both_weights = jnp.concatenate([gate_matrix[0], up_matrix[0]], axis=1).reshape(
        tp_count, part_width, 2 * hidden_dev
    )
    down_blocks = down_matrix[0].reshape(hidden_dev, tp_count, part_width)
    both_pre = lax.dot_general(
        token_blocks, both_weights, (((0, 2), (0, 1)), ((), ())), preferred_element_type=jnp.float32
    )
    gate_pre = both_pre[:, :hidden_dev]
    up_pre = both_pre[:, hidden_dev:]
    sigmoid_gate = jax.nn.sigmoid(gate_pre)
    activated = gate_pre * sigmoid_gate
    hidden = activated * up_pre
    back_grad = lax.dot_general(
        grad_blocks, down_blocks, (((0, 2), (1, 2)), ((), ())), preferred_element_type=jnp.float32
    )
    gate_grad = (
        back_grad * up_pre * sigmoid_gate * (1.0 + gate_pre * (1.0 - sigmoid_gate))
    ).astype(jnp.bfloat16)
    up_grad = (back_grad * activated).astype(jnp.bfloat16)
    both_grad = jnp.concatenate([gate_grad, up_grad], axis=1)
    hidden_low = hidden.astype(jnp.bfloat16)
    down_full = lax.dot_general(
        hidden_low, grad_blocks, (((0,), (1,)), ((), ())), preferred_element_type=jnp.float32
    ).reshape(hidden_dev, full_width)
    both_full = lax.dot_general(
        token_blocks, both_grad, (((1,), (0,)), ((), ())), preferred_element_type=jnp.float32
    ).reshape(full_width, 2 * hidden_dev)
    gate_full = both_full[:, :hidden_dev]
    up_full = both_full[:, hidden_dev:]
    scores = jnp.sum(hidden * back_grad, axis=1)
    partial_rows = lax.dot_general(
        both_grad, both_weights, (((1,), (2,)), ((), ())), preferred_element_type=jnp.float32
    ).astype(jnp.bfloat16)
    pieces = lax.all_to_all(partial_rows, "tp", split_axis=1, concat_axis=1, tiled=True)
    summed = jnp.sum(pieces, axis=1, dtype=jnp.float32).reshape(sources, capacity, part_width)
    norm_terms = jnp.stack(
        [jnp.sum(gate_full * gate_full, axis=1), jnp.sum(up_full * up_full, axis=1)]
    )
    scores_all, norms_all = in_one((scores.reshape(sources, capacity), norm_terms), "tp")
    back_rows, back_scores = sent_together_2((summed, scores_all), "ep", 0, 0, 2)
    pair_rows = jnp.sum(back_rows.reshape(experts, 2, capacity, part_width), axis=1).reshape(
        experts * capacity, part_width
    )
    token_gradient = jnp.sum(
        jnp.take(pair_rows, target, axis=0).reshape(tok_rows, top_count, part_width), axis=1
    ).astype(jnp.bfloat16)
    pair_scores = jnp.sum(back_scores.reshape(experts, 2, capacity), axis=1).reshape(
        experts * capacity
    )
    mixing_gradient = jnp.take(pair_scores, target, axis=0).reshape(tok_rows, top_count) / mixing
    down_norms = jnp.sum(down_full * down_full, axis=1)
    return (
        token_gradient,
        mixing_gradient,
        gate_full.astype(jnp.bfloat16)[None],
        up_full.astype(jnp.bfloat16)[None],
        down_full.astype(jnp.bfloat16)[None],
        norms_all[None],
        down_norms[None],
    )


def solution(mesh):
    placed = (
        P("ep", "tp"),
        P("ep", None),
        P("ep", None),
        P("ep", None, "tp"),
        P("ep", None, "tp"),
        P("ep", "tp", None),
        P("ep", "tp"),
    )
    return jax.shard_map(
        on_device,
        mesh=mesh,
        in_specs=placed,
        out_specs=(
            P("ep", "tp"),
            P("ep", None),
            P("ep", None, "tp"),
            P("ep", None, "tp"),
            P("ep", "tp", None),
            P("ep", None, None),
            P("ep", "tp"),
        ),
        check_vma=False,
    )
```

profile of v0, /device:TPU:1, one launch (start us, length us, event | category | flops | bytes accessed | tf_op | source)
XLA Modules:
  0.0 333.7 jit_solution(7546690937035001095)
XLA Ops:
  11.9 71.5 %all_to_all.21 = bf16[64,10,128]{2,1,0:T(8,128)(2,1)S(1)} all-to-all(bf16[64,10,128]{2,1,0:T(8,128)(2,1)S(1)} %pad_maximum_fusion.5), channel_id=1, replica_groups=mesh['ep'=64,'tp'=16] {'ep'}, dimensions={0} | all-to-all | bytes 327680 | tf_op jit(solution)/shard_map/all_to_all | solution.py:10
  84.2 63.7 %all-gather.2.cloned.1.call-done = bf16[16,128,5,128]{3,1,2,0:T(8,128)(2,1)} async-done(((bf16[1,128,5,128]{3,1,2,0:T(8,128)(2,1)}), bf16[16,128,5,128]{3,1,2,0:T(8,128)(2,1)}) %all-gather.2.cloned.1.call-update) | async-done | bytes 2621456 | tf_op jit(solution)/shard_map/all_gather | solution.py:20
  147.9 2.3 fusion.29
  150.2 3.9 %collective-permute-start = (bf16[16,64,5,128]{3,1,2,0:T(8,128)(2,1)S(1)}, bf16[16,64,5,128]{3,1,2,0:T(8,128)(2,1)}, u32[]{:S(2)}, u32[]{:S(2)}) collective-permute-start(bf16[16,64,5,128]{3,1,2,0:T(8,128)(2,1)S(1)} %get-tuple-element.46), channel_id=1, source_target_pairs={{0,16},{16,0},{32,48},{48,32},{64,80},{80,64},{96,112},{112,96},{1... | collective-permute-start | bytes 3932168 | tf_op jit(solution)/shard_map/ppermute | solution.py:30
  154.1 1.9 collective-permute-start.1
  156.1 1.0 copy.113
  157.1 2.0 copy.114
  159.1 1.9 copy.135
  162.8 2.2 copy.105
  165.0 2.2 copy.111
  167.1 2.0 maximum_select_fusion
  169.1 5.4 %copy.118 = bf16[16,128,640]{2,1,0:T(8,128)(2,1)} copy(bf16[16,128,640]{1,0,2:T(8,128)(2,1)} %bitcast.69) | data formatting | bytes 5242880 | tf_op jit(solution)/shard_map/dot_general | solution.py:146
  174.6 2.9 fusion.4
  177.5 1.0 multiply_reduce_fusion.3
  179.5 1.0 fusion.15
  181.6 4.5 %all-to-all-start.2 = ((f32[16,1,4736]{2,1,0:T(1,128)}), f32[16,1,4736]{2,1,0:T(1,128)S(1)}, u32[]{:S(2)}, u32[]{:S(2)}) async-start(f32[16,1,4736]{2,1,0:T(1,128)} %broadcast_in_dim.54), calls=%async_computation.2 | async-start | bytes 606208 | tf_op jit(solution)/shard_map/all_to_all | solution.py:35
  186.1 3.5 %convolution_convert_fusion = bf16[640,16,128]{2,0,1:T(8,128)(2,1)} fusion(bf16[16,128,128]{1,2,0:T(8,128)(2,1)} %copy.114, bf16[16,128,128]{1,2,0:T(8,128)(2,1)S(1)} %copy-done.4, bf16[640,128]{0,1:T(8,128)(2,1)S(1)} %get-tuple-element.53, bf16[640,128]{0,1:T(8,128)(2,1)} %copy-done.6), kind=kOutput, calls=%fused_computation.9 | convolution fusion | flops 675151872 | bytes 3997696 | tf_op jit(solution)/shard_map/dot_general | solution.py:152
  189.6 4.9 %all-to-all-done.2 = f32[16,1,4736]{2,1,0:T(1,128)S(1)} async-done(((f32[16,1,4736]{2,1,0:T(1,128)}), f32[16,1,4736]{2,1,0:T(1,128)S(1)}, u32[]{:S(2)}, u32[]{:S(2)}) %all-to-all-start.2) | async-done | bytes 303136 | tf_op jit(solution)/shard_map/all_to_all | solution.py:35
  194.6 4.4 %all-to-all-start.1 = ((bf16[640,16,128]{2,0,1:T(8,128)(2,1)}), bf16[640,16,128]{2,0,1:T(8,128)(2,1)}, u32[]{:S(2)}, u32[]{:S(2)}) async-start(bf16[640,16,128]{2,0,1:T(8,128)(2,1)} %convolution_convert_fusion), calls=%async_computation.1 | async-start | bytes 5242880 | tf_op jit(solution)/shard_map/all_to_all | solution.py:155
  199.2 1.0 reshape_reshape.8
  200.2 35.4 %all-to-all-done.1 = bf16[640,16,128]{2,0,1:T(8,128)(2,1)} async-done(((bf16[640,16,128]{2,0,1:T(8,128)(2,1)}), bf16[640,16,128]{2,0,1:T(8,128)(2,1)}, u32[]{:S(2)}, u32[]{:S(2)}) %all-to-all-start.1) | async-done | bytes 2621472 | tf_op jit(solution)/shard_map/all_to_all | solution.py:155
  235.7 2.1 convert_reduce_fusion
  238.6 1.3 pad_maximum_fusion.1
  239.9 1.7 reshape.181
  241.6 26.0 %all-to-all-start.3 = ((f32[64,1,1290]{2,1,0:T(1,128)}), f32[64,1,1290]{2,1,0:T(1,128)}, u32[]{:S(2)}, u32[]{:S(2)}) async-start(f32[64,1,1290]{2,1,0:T(1,128)} %reshape.181), calls=%async_computation.3 | async-start | bytes 720896 | tf_op jit(solution)/shard_map/all_to_all | solution.py:57
  267.9 4.9 %copy.122 = bf16[16,128,640]{2,1,0:T(8,128)(2,1)} copy(bf16[16,128,640]{1,0,2:T(8,128)(2,1)} %bitcast.68) | data formatting | bytes 5242880 | tf_op jit(solution)/shard_map/dot_general | solution.py:143
  272.9 1.0 copy.124
  273.9 1.0 copy.125
  274.9 4.2 %multiply_reduce_fusion = (f32[128]{0:T(128)}, bf16[1,128,2048]{2,1,0:T(8,128)(2,1)}) fusion(bf16[2048,640]{1,0:T(8,128)(2,1)} %bitcast.71, f32[640,256]{0,1:T(8,128)} %copy-done.7), kind=kOutput, calls=%fused_computation.16 | convolution fusion | flops 336822144 | bytes 3801600 | tf_op jit(solution)/shard_map/dot_general | solution.py:143
  279.8 38.3 %all-to-all-done.3 = f32[64,1,1290]{2,1,0:T(1,128)} async-done(((f32[64,1,1290]{2,1,0:T(1,128)}), f32[64,1,1290]{2,1,0:T(1,128)}, u32[]{:S(2)}, u32[]{:S(2)}) %all-to-all-start.3) | async-done | bytes 330272 | tf_op jit(solution)/shard_map/all_to_all | solution.py:57
  318.6 2.5 reduce.5
  322.4 1.9 gather_fusion.1
  (72 shorter events, 15.5 us)
Async XLA Ops:
  7.2 4.2 %copy-start = (bf16[128,128]{1,0:T(8,128)(2,1)S(1)}, bf16[128,128]{1,0:T(8,128)(2,1)}, u32[]{:S(2)}) copy-start(bf16[128,128]{1,0:T(8,128)(2,1)} %param.7) | copy-start | bytes 98308
  7.2 140.7 %all-gather.2.cloned.1.call-start = ((), (), s32[]{:S(2)}) async-start(), calls=%async_computation.4 | async-start | bytes 2785280 | tf_op jit(solution)/shard_map/all_gather | solution.py:20
  84.2 71.8 %copy-start.3 = (bf16[1,2048,128]{2,1,0:T(8,128)(2,1)S(1)}, bf16[1,2048,128]{2,1,0:T(8,128)(2,1)}, u32[]{:S(2)}) copy-start(bf16[1,2048,128]{2,1,0:T(8,128)(2,1)} %param.10) | copy-start | bytes 1572868
  150.2 12.5 %collective-permute-start = (bf16[16,64,5,128]{3,1,2,0:T(8,128)(2,1)S(1)}, bf16[16,64,5,128]{3,1,2,0:T(8,128)(2,1)}, u32[]{:S(2)}, u32[]{:S(2)}) collective-permute-start(bf16[16,64,5,128]{3,1,2,0:T(8,128)(2,1)S(1)} %get-tuple-element.46), channel_id=1, source_target_pairs={{0,16},{16,0},{32,48},{48,32},{64,80},{80,64},{96,112},{112,96},{1... | collective-permute-start | bytes 3932168 | tf_op jit(solution)/shard_map/ppermute | solution.py:30
  154.1 10.8 %collective-permute-start.1 = (bf16[16,64,5,128]{3,1,2,0:T(8,128)(2,1)S(1)}, bf16[16,64,5,128]{3,1,2,0:T(8,128)(2,1)}, u32[]{:S(2)}, u32[]{:S(2)}) collective-permute-start(bf16[16,64,5,128]{3,1,2,0:T(8,128)(2,1)S(1)} %get-tuple-element.47), channel_id=1, source_target_pairs={{0,16},{16,0},{32,48},{48,32},{64,80},{80,64},{96,112},{112,96},{1... | collective-permute-start | bytes 3932168 | tf_op jit(solution)/shard_map/ppermute | solution.py:30
  169.1 8.4 %copy-start.2 = (bf16[16,64,10,128]{3,0,2,1:T(8,128)(2,1)}, bf16[16,64,10,128]{3,0,2,1:T(8,128)(2,1)S(1)}, u32[]{:S(2)}) copy-start(bf16[16,64,10,128]{3,0,2,1:T(8,128)(2,1)S(1)} %get-tuple-element.57) | copy-start | bytes 7864324
  169.1 5.5 %copy-start.4 = (bf16[16,128,128]{1,2,0:T(8,128)(2,1)S(1)}, bf16[16,128,128]{1,2,0:T(8,128)(2,1)}, u32[]{:S(2)}) copy-start(bf16[16,128,128]{1,2,0:T(8,128)(2,1)} %copy.113) | copy-start | bytes 1572868
  174.6 2.9 copy-start.5
  177.5 1.1 copy-start.7
  177.5 2.0 copy-start.1
  178.5 1.9 copy-start.6
  181.6 13.0 %all-to-all-start.2 = ((f32[16,1,4736]{2,1,0:T(1,128)}), f32[16,1,4736]{2,1,0:T(1,128)S(1)}, u32[]{:S(2)}, u32[]{:S(2)}) async-start(f32[16,1,4736]{2,1,0:T(1,128)} %broadcast_in_dim.54), calls=%async_computation.2 | async-start | bytes 606208 | tf_op jit(solution)/shard_map/all_to_all | solution.py:35
  194.6 41.1 %all-to-all-start.1 = ((bf16[640,16,128]{2,0,1:T(8,128)(2,1)}), bf16[640,16,128]{2,0,1:T(8,128)(2,1)}, u32[]{:S(2)}, u32[]{:S(2)}) async-start(bf16[640,16,128]{2,0,1:T(8,128)(2,1)} %convolution_convert_fusion), calls=%async_computation.1 | async-start | bytes 5242880 | tf_op jit(solution)/shard_map/all_to_all | solution.py:155
  241.6 76.5 %all-to-all-start.3 = ((f32[64,1,1290]{2,1,0:T(1,128)}), f32[64,1,1290]{2,1,0:T(1,128)}, u32[]{:S(2)}, u32[]{:S(2)}) async-start(f32[64,1,1290]{2,1,0:T(1,128)} %reshape.181), calls=%async_computation.3 | async-start | bytes 720896 | tf_op jit(solution)/shard_map/all_to_all | solution.py:57
Sparse Core Ops, SparseCore 0:
  84.3 63.4 all-gather.1
where the time goes:
time: 335 us; the launch traced here: 334 us
  waiting for transfers between devices  142 us (42%)
  blocking collectives  71.5 us (21%)
  local copies, waits for them, and re-layouts  41.1 us (12%)
  starting transfers between devices  40.8 us (12%)
  between operations  14.5 us (4%)
  matrix products  13.3 us (4%)
  other arithmetic  10.2 us (3%)
    all_to_all x1, blocking collectives, side_by_side(): lax.all_to_all(both, axis, split_axis=split_dim, concat_axis=concat_dim,...  71.5 us
    all_gather x1, waiting for transfers between devices, sent_together(): lax.all_gather(both, axis, axis=dim, tiled=True)  63.7 us
    all_to_all x1, waiting for transfers between devices, sent_together_2(): lax.all_to_all(both, axis, split_axis=split_dim, concat_axis=concat_dim,...  38.3 us
    all_to_all x1, waiting for transfers between devices, on_device(): lax.all_to_all(partial_rows, 'tp', split_axis=1, concat_axis=1, tiled=True)  35.4 us
    all_to_all x1, starting transfers between devices, sent_together_2(): lax.all_to_all(both, axis, split_axis=split_dim, concat_axis=concat_dim,...  26 us
    unnamed x27, local copies, waits for them, and re-layouts  11.4 us
  transfers between devices with their start and end apart: 6, of which 4 were waited for; matrix products, arithmetic and copies ran while one was open for 8% of the time, Pallas kernels for 0%

commit v1 on v0

v1 whole, which is shorter than its diff:
```python
import functools

import jax
import jax.numpy as jnp
from jax import lax
from jax.experimental import pallas as pl
from jax.experimental.pallas import tpu as pltpu
from jax.sharding import PartitionSpec as P

MESH = pl.DeviceIdType.MESH
F32 = jnp.float32
BF16 = jnp.bfloat16
NY = NX = 4
NT = NY * NX
NZ = 32
CAP = 10
GROUP = 8
NQ = NZ // GROUP
HALF = GROUP * CAP
ROWS = 2 * HALF
ALL = NQ * ROWS
SEND = 24
BACK = 16
LANES = 128


def offset_of(place):
    return (place + 1) // 2 if place % 2 else -(place // 2)


def opposite(place):
    if place in (0, NZ - 1):
        return place
    return place + 1 if place % 2 else place - 1


def dot(a, b, dims):
    return lax.dot_general(a, b, (dims, ((), ())), preferred_element_type=F32)


def iota(shape, dim):
    return lax.broadcasted_iota(jnp.int32, shape, dim)


def tenth(value):
    return ((value.astype(F32) + 0.5) * (1.0 / CAP)).astype(jnp.int32)


def body(
    tokens,
    upstream,
    routing,
    mixing,
    mixing_rows,
    gate_hbm,
    up_hbm,
    down_hbm,
    token_out,
    mixing_out,
    gate_out,
    up_out,
    down_out,
    norms_out,
    down_norms_out,
    w_in,
    w_down,
    z_send,
    z_recv,
    x_all,
    y_all,
    grads,
    hidden_all,
    part,
    part_in,
    part_sum,
    part_recv,
    score_own,
    score_in,
    score_sum,
    score_recv,
    back_send,
    back_recv,
    gate_full,
    up_full,
    down_full,
    norms,
    norms_recv,
    sem_w,
    sem_out,
    sem_send,
    sem_z,
    sem_first,
    sem_second,
    sem_core,
    sem_part,
    sem_score,
    sem_sum,
    sem_sum_score,
    sem_back,
    sem_norm,
):
    ep = lax.axis_index("ep")
    tp = lax.axis_index("tp")
    z, core = ep // 2, ep % 2
    y, x = tp // NX, tp % NX

    def at_z(offset):
        return (lax.rem(z + offset + NZ, NZ) * 2 + core, tp)

    def at_plane(dy, dx):
        return (ep, lax.rem(y + dy, NY) * NX + lax.rem(x + dx, NX))

    partner = (z * 2 + 1 - core, tp)
    plane = [(dy, dx) for dy in range(NY) for dx in range(NX) if (dy, dx) != (0, 0)]

    def send(source, target, stage, arrival, device):
        pltpu.make_async_remote_copy(
            src_ref=source,
            dst_ref=target,
            send_sem=sem_send.at[stage],
            recv_sem=arrival,
            device_id=device,
            device_id_type=MESH,
        ).start()

    def await_bytes(ref, sem):
        pltpu.make_async_copy(ref, ref, sem).wait()

    weights = [
        pltpu.make_async_copy(gate_hbm.at[0], w_in.at[:, pl.ds(0, LANES)], sem_w.at[0]),
        pltpu.make_async_copy(up_hbm.at[0], w_in.at[:, pl.ds(LANES, LANES)], sem_w.at[1]),
        pltpu.make_async_copy(down_hbm.at[0], w_down, sem_w.at[2]),
    ]
    for copy in weights:
        copy.start()

    barrier = pltpu.get_barrier_semaphore()
    for offset in range(1, NZ):
        pl.semaphore_signal(barrier, inc=1, device_id=at_z(offset), device_id_type=MESH)
    for dy, dx in plane:
        pl.semaphore_signal(barrier, inc=1, device_id=at_plane(dy, dx), device_id_type=MESH)
    pl.semaphore_signal(barrier, inc=1, device_id=partner, device_id_type=MESH)

    block = tokens.shape[0]
    upper = (iota((block, block), 0) < iota((block, block), 1)).astype(BF16)
    experts = iota((NZ, block), 0)
    chosen = [(routing[k : k + 1, :] == experts).astype(F32) for k in range(2)]
    earlier = [dot(c.astype(BF16), upper, ((1,), (0,))) for c in chosen]
    earlier[1] = earlier[1] + jnp.sum(chosen[0], axis=1, keepdims=True)
    places, slots = [], []
    for k in range(2):
        slots.append(jnp.sum(chosen[k] * earlier[k], axis=0, keepdims=True).astype(jnp.int32))
        ahead = routing[k : k + 1, :] - z
        ahead = jnp.where(ahead < 0, ahead + NZ, ahead)
        places.append(
            jnp.where(
                ahead == 0,
                0,
                jnp.where(ahead <= NZ // 2, 2 * ahead - 1, 2 * (NZ - ahead)),
            )
        )
    rows_out = iota((NZ * SEND, block), 0)
    token_hot, grad_hot = [], []
    for k in range(2):
        target = places[k] * SEND + slots[k]
        token_hot.append(rows_out == target)
        grad_hot.append((rows_out == target + CAP).astype(BF16))
    placed = dot((token_hot[0] | token_hot[1]).astype(BF16), tokens[...], ((1,), (0,)))
    cotangent = upstream[...].astype(F32)
    for k in range(2):
        scaled = (mixing[:, k : k + 1] * cotangent).astype(BF16)
        placed = placed + dot(grad_hot[k], scaled, ((1,), (0,)))
    z_send[...] = placed.reshape(NZ * SEND // 8, 8, LANES).astype(BF16)
    tiles = SEND // 8
    z_recv[0:tiles] = z_send[0:tiles]

    pl.semaphore_wait(barrier, NZ - 1 + len(plane) + 1)

    for place in range(1, NZ):
        send(
            z_send.at[pl.ds(place * tiles, tiles)],
            z_recv.at[pl.ds(opposite(place) * tiles, tiles)],
            0,
            sem_z.at[opposite(place) // GROUP],
            at_z(offset_of(place)),
        )

    row = iota((ROWS, GROUP * SEND), 0)
    col = iota((ROWS, GROUP * SEND), 1)
    low = row < HALF
    pair = jnp.where(low, row, row - HALF)
    source = tenth(pair)
    pick = (source * SEND + (pair - source * CAP) + jnp.where(low, 0, CAP) == col).astype(BF16)

    row = iota((GROUP * BACK, HALF), 0)
    col = iota((GROUP * BACK, HALF), 1)
    within = row % BACK
    spread = ((row // BACK * CAP + within == col) & (within < CAP)).astype(BF16)
    back_row = iota((GROUP * BACK, LANES), 0) % BACK

    for copy in weights:
        copy.wait()

    def own_rows(q):
        return pl.ds(pl.multiple_of(q * ROWS + core * HALF, 16), HALF)

    def other_rows(q):
        return pl.ds(pl.multiple_of(q * ROWS + (1 - core) * HALF, 16), HALF)

    def stage_gather_first(q):
        count = GROUP * tiles
        if q == 0:
            await_bytes(z_recv.at[pl.ds(tiles, count - tiles)], sem_z.at[0])
        else:
            await_bytes(z_recv.at[pl.ds(q * count, count)], sem_z.at[q])
        arrived = z_recv[pl.ds(q * count, count)].astype(F32).reshape(GROUP * SEND, LANES)
        rows = dot(pick, arrived.astype(BF16), ((1,), (0,))).astype(BF16)
        x_all[y, x, own_rows(q), :] = rows[:HALF]
        y_all[y, x, own_rows(q), :] = rows[HALF:]
        for d in range(1, NX):
            mine = x_all.at[y, x, own_rows(q), :]
            send(mine, mine, 1, sem_first.at[q, 0, d - 1], at_plane(0, d))
        for d in range(1, NY):
            mine = y_all.at[y, x, own_rows(q), :]
            send(mine, mine, 1, sem_first.at[q, 1, d - 1], at_plane(d, 0))

    def stage_gather_second(q):
        for d in range(1, NX):
            await_bytes(x_all.at[y, x, own_rows(q), :], sem_first.at[q, 0, d - 1])
        for d in range(1, NY):
            mine = x_all.at[y, :, own_rows(q), :]
            send(mine, mine, 2, sem_second.at[q, 0, d - 1], at_plane(d, 0))
        for d in range(1, NY):
            await_bytes(y_all.at[y, x, own_rows(q), :], sem_first.at[q, 1, d - 1])
        for d in range(1, NX):
            mine = y_all.at[:, x, own_rows(q), :]
            send(mine, mine, 2, sem_second.at[q, 1, d - 1], at_plane(0, d))

    def stage_cores(q):
        for d in range(1, NY):
            await_bytes(x_all.at[y, :, own_rows(q), :], sem_second.at[q, 0, d - 1])
        mine = x_all.at[:, :, own_rows(q), :]
        send(mine, mine, 3, sem_core.at[q, 0], partner)
        for d in range(1, NX):
            await_bytes(y_all.at[:, x, own_rows(q), :], sem_second.at[q, 1, d - 1])
        mine = y_all.at[:, :, own_rows(q), :]
        send(mine, mine, 3, sem_core.at[q, 1], partner)

    def stage_compute(q):
        rows = pl.ds(q * ROWS, ROWS)
        await_bytes(x_all.at[:, :, other_rows(q), :], sem_core.at[q, 0])
        x_rows = jnp.concatenate(
            [x_all[i, j, rows, :] for i in range(NY) for j in range(NX)], axis=1
        )
        pre = dot(x_rows, w_in[...], ((1,), (0,)))
        await_bytes(y_all.at[:, :, other_rows(q), :], sem_core.at[q, 1])
        y_rows = jnp.concatenate(
            [y_all[i, j, rows, :] for i in range(NY) for j in range(NX)], axis=1
        )
        back = dot(y_rows, w_down[...], ((1,), (1,)))
        gate_pre, up_pre = pre[:, :LANES], pre[:, LANES:]
        sig = jax.nn.sigmoid(gate_pre)
        act = gate_pre * sig
        hidden = act * up_pre
        gate_grad = (back * up_pre * sig * (1.0 + gate_pre * (1.0 - sig))).astype(BF16)
        up_grad = (back * act).astype(BF16)
        both = jnp.concatenate([gate_grad, up_grad], axis=1)
        grads[rows, :] = both
        hidden_all[rows, :] = hidden.astype(BF16)
        scores = jnp.sum(jnp.transpose(hidden * back), axis=0, keepdims=True)
        pad = jnp.zeros((1, LANES - HALF), F32)
        for half in range(2):
            score_own[q, half] = jnp.concatenate(
                [scores[:, half * HALF : (half + 1) * HALF], pad], axis=1
            )
        for b in range(NT // 2):
            term = dot(both, w_in[pl.ds(b * 2 * LANES, 2 * LANES), :], ((1,), (1,)))
            term = term.astype(BF16)
            for h in range(2):
                t = 2 * b + h
                part[t // NX, t % NX, rows, :] = term[:, h * LANES : (h + 1) * LANES]
        send(
            part.at[:, :, other_rows(q), :],
            part_in.at[q],
            4,
            sem_part.at[q],
            partner,
        )
        send(score_own.at[q, 1 - core], score_in.at[q], 5, sem_score.at[q], partner)

    def stage_pair_sum(q):
        await_bytes(part_in.at[q], sem_part.at[q])
        await_bytes(score_in.at[q], sem_score.at[q])
        total = part[:, :, own_rows(q), :].astype(F32) + part_in[q].astype(F32)
        part_sum[q] = total.astype(BF16)
        score_sum[q] = score_own[q, core] + score_in[q]
        for n, (dy, dx) in enumerate(plane):
            send(
                part_sum.at[q, lax.rem(y + dy, NY), lax.rem(x + dx, NX)],
                part_recv.at[q, n],
                6,
                sem_sum.at[q],
                at_plane(dy, dx),
            )
            send(score_sum.at[q], score_recv.at[q, n], 7, sem_sum_score.at[q], at_plane(dy, dx))

    def stage_back(q):
        await_bytes(part_recv.at[q], sem_sum.at[q])
        await_bytes(score_recv.at[q], sem_sum_score.at[q])
        total = part_sum[q, y, x].astype(F32)
        score = score_sum[q]
        for n in range(len(plane)):
            total = total + part_recv[q, n].astype(F32)
            score = score + score_recv[q, n]
        high = score.astype(BF16)
        rest = score - high.astype(F32)
        middle = rest.astype(BF16)
        low_bits = (rest - middle.astype(F32)).astype(BF16)
        message = dot(spread, total.astype(BF16), ((1,), (0,)))
        for n, piece in enumerate((high, middle, low_bits)):
            message = jnp.where(back_row == CAP + n, piece.astype(F32), message)
        message = message.astype(BF16)
        back_send[pl.ds(q * GROUP * BACK, GROUP * BACK), :] = message
        if q == 0:
            back_recv[0:BACK, :] = message[:BACK]
        for place in range(q * GROUP, (q + 1) * GROUP):
            if place:
                send(
                    back_send.at[pl.ds(place * BACK, BACK), :],
                    back_recv.at[pl.ds(opposite(place) * BACK, BACK), :],
                    8,
                    sem_back,
                    at_z(offset_of(place)),
                )

    def weight_in():
        def step(b, _):
            x_rows = x_all[b // NX, b % NX]
            full = dot(x_rows, grads[...], ((0,), (0,)))
            at = pl.ds(pl.multiple_of(b * LANES, LANES), LANES)
            gate_full[at, :] = full[:, :LANES].astype(BF16)
            up_full[at, :] = full[:, LANES:].astype(BF16)
            for h in range(2):
                piece = full[:, h * LANES : (h + 1) * LANES]
                norms[h : h + 1, at] = jnp.sum(
                    jnp.transpose(piece * piece), axis=0, keepdims=True
                )
            return 0

        lax.fori_loop(0, NT, step, 0)
        pltpu.make_async_copy(gate_full, gate_out.at[0], sem_out.at[0]).start()
        pltpu.make_async_copy(up_full, up_out.at[0], sem_out.at[1]).start()
        for n, (dy, dx) in enumerate(plane):
            send(norms, norms_recv.at[n], 9, sem_norm, at_plane(dy, dx))

    def weight_down():
        hidden_t = jnp.transpose(hidden_all[...].astype(F32)).astype(BF16)

        def step(b, squares):
            y_rows = jnp.concatenate(
                [y_all[b // 2, 2 * (b % 2)], y_all[b // 2, 2 * (b % 2) + 1]], axis=1
            )
            full = dot(hidden_t, y_rows, ((1,), (0,)))
            at = pl.ds(pl.multiple_of(b * 2 * LANES, 2 * LANES), 2 * LANES)
            down_full[:, at] = full.astype(BF16)
            left, right = full[:, :LANES], full[:, LANES:]
            return squares + left * left + right * right

        squares = lax.fori_loop(0, NT // 2, step, jnp.zeros((LANES, LANES), F32))
        down_norms_out[...] = jnp.sum(jnp.transpose(squares), axis=0, keepdims=True)
        pltpu.make_async_copy(down_full, down_out.at[0], sem_out.at[2]).start()

    stages = (
        (5, stage_back),
        (4, stage_pair_sum),
        (0, stage_gather_first),
        (1, stage_gather_second),
        (3, stage_compute),
        (2, stage_cores),
    )
    for step in range(NQ + 5):
        if step == NQ + 4:
            weight_in()
        for depth, stage in stages:
            if 0 <= step - depth < NQ:
                stage(step - depth)
    weight_down()

    await_bytes(back_recv.at[pl.ds(BACK, (NZ - 1) * BACK), :], sem_back)
    rows_back = iota((NZ * BACK, block), 0)
    returned = back_recv[...]
    row_hot = None
    for k in range(2):
        start = places[k] * BACK
        hot = rows_back == start + slots[k]
        row_hot = hot if row_hot is None else row_hot | hot
        score_hot = (rows_back >= start + CAP) & (rows_back < start + CAP + 3)
        mirrored = jnp.where(
            (places[k] == 0) | (places[k] == NZ - 1),
            places[k],
            jnp.where(places[k] % 2 == 1, places[k] + 1, places[k] - 1),
        )
        lane = mirrored % GROUP * CAP + slots[k]
        lines = dot(returned, score_hot.astype(BF16), ((0,), (0,)))
        score = jnp.sum(
            jnp.where(iota((LANES, block), 0) == lane, lines, 0.0), axis=0, keepdims=True
        )
        mixing_out[k : k + 1, :] = score / mixing_rows[k : k + 1, :]
    token_out[...] = dot(row_hot.astype(BF16), returned, ((0,), (0,))).astype(BF16)

    await_bytes(norms_recv, sem_norm)
    total = norms[...]
    for n in range(len(plane)):
        total = total + norms_recv[n]
    norms_out[0] = total

    for full, out, n in ((gate_full, gate_out, 0), (up_full, up_out, 1), (down_full, down_out, 2)):
        pltpu.make_async_copy(full, out.at[0], sem_out.at[n]).wait()
    sent = (
        z_recv.at[pl.ds(tiles, (NZ - 1) * tiles)],
        x_all.at[0, pl.ds(0, 3)],
        x_all.at[pl.ds(0, 3)],
        x_all,
        x_all.at[pl.ds(0, 2)],
        score_in,
        part_recv,
        score_recv,
        back_recv.at[pl.ds(BACK, (NZ - 1) * BACK), :],
        norms_recv,
    )
    for n, ref in enumerate(sent):
        await_bytes(ref, sem_send.at[n])


def on_device(tokens, routing, mixing, gate_matrix, up_matrix, down_matrix, upstream):
    vmem = pl.BlockSpec(memory_space=pltpu.VMEM)
    hbm = pl.BlockSpec(memory_space=pl.ANY)
    block = tokens.shape[0]
    shape = jax.ShapeDtypeStruct
    dma = pltpu.SemaphoreType.DMA
    results = pl.pallas_call(
        body,
        out_shape=(
            shape((block, LANES), BF16),
            shape((2, block), F32),
            shape(gate_matrix.shape, BF16),
            shape(up_matrix.shape, BF16),
            shape(down_matrix.shape, BF16),
            shape((1, 2, NT * LANES), F32),
            shape((1, LANES), F32),
        ),
        in_specs=[vmem] * 5 + [hbm] * 3,
        out_specs=(vmem, vmem, hbm, hbm, hbm, vmem, vmem),
        scratch_shapes=[
            pltpu.VMEM((NT * LANES, 2 * LANES), BF16),
            pltpu.VMEM((LANES, NT * LANES), BF16),
            pltpu.VMEM((NZ * SEND // 8, 8, LANES), BF16),
            pltpu.VMEM((NZ * SEND // 8, 8, LANES), BF16),
            pltpu.VMEM((NY, NX, ALL, LANES), BF16),
            pltpu.VMEM((NY, NX, ALL, LANES), BF16),
            pltpu.VMEM((ALL, 2 * LANES), BF16),
            pltpu.VMEM((ALL, LANES), BF16),
            pltpu.VMEM((NY, NX, ALL, LANES), BF16),
            pltpu.VMEM((NQ, NY, NX, HALF, LANES), BF16),
            pltpu.VMEM((NQ, NY, NX, HALF, LANES), BF16),
            pltpu.VMEM((NQ, NT - 1, HALF, LANES), BF16),
            pltpu.VMEM((NQ, 2, 1, LANES), F32),
            pltpu.VMEM((NQ, 1, LANES), F32),
            pltpu.VMEM((NQ, 1, LANES), F32),
            pltpu.VMEM((NQ, NT - 1, 1, LANES), F32),
            pltpu.VMEM((NZ * BACK, LANES), BF16),
            pltpu.VMEM((NZ * BACK, LANES), BF16),
            pltpu.VMEM((NT * LANES, LANES), BF16),
            pltpu.VMEM((NT * LANES, LANES), BF16),
            pltpu.VMEM((LANES, NT * LANES), BF16),
            pltpu.VMEM((2, NT * LANES), F32),
            pltpu.VMEM((NT - 1, 2, NT * LANES), F32),
            dma((3,)),
            dma((3,)),
            dma((10,)),
            dma((NQ,)),
            dma((NQ, 2, 3)),
            dma((NQ, 2, 3)),
            dma((NQ, 2)),
            dma((NQ,)),
            dma((NQ,)),
            dma((NQ,)),
            dma((NQ,)),
            dma,
            dma,
        ],
        compiler_params=pltpu.CompilerParams(
            collective_id=0, has_side_effects=True, vmem_limit_bytes=56 * 1024 * 1024
        ),
    )(
        tokens,
        upstream,
        routing.T,
        mixing,
        mixing.T,
        gate_matrix,
        up_matrix,
        down_matrix,
    )
    token_gradient, mixing_t, gate, up, down, norms, down_norms = results
    return token_gradient, mixing_t.T, gate, up, down, norms, down_norms


def solution(mesh):
    placed = (
        P("ep", "tp"),
        P("ep", None),
        P("ep", None),
        P("ep", None, "tp"),
        P("ep", None, "tp"),
        P("ep", "tp", None),
        P("ep", "tp"),
    )
    return jax.shard_map(
        on_device,
        mesh=mesh,
        in_specs=placed,
        out_specs=(
            P("ep", "tp"),
            P("ep", None),
            P("ep", None, "tp"),
            P("ep", None, "tp"),
            P("ep", "tp", None),
            P("ep", None, None),
            P("ep", "tp"),
        ),
        check_vma=False,
    )
```

time: 335 us -> 113 us (0.34)
  waiting for transfers between devices: 142 us -> 0 us
  Pallas kernels: 0 us -> 102 us
  blocking collectives: 71.5 us -> 0 us
  starting transfers between devices: 40.8 us -> 0 us
  local copies, waits for them, and re-layouts: 41.1 us -> 8.43 us
  between operations: 14.5 us -> 0.66 us
  matrix products: 13.3 us -> 0 us
  other arithmetic: 10.2 us -> 0 us
    pallas_call x0 -> x1, Pallas kernels: none -> 102 us  [on_device(): pl.pallas_call(body, out_shape=(shape((block, LANES), BF16), shape((2, bl...]
    all_to_all x3 -> x0, waiting for transfers between devices: 78.7 us -> none  [the longest x1 38.3 us: sent_together_2(): lax.all_to_all(both, axis, split_axis=split_dim, concat_axis=concat_dim,...]
    all_to_all x1 -> x0, blocking collectives: 71.5 us -> none  [side_by_side(): lax.all_to_all(both, axis, split_axis=split_dim, concat_axis=concat_dim,...]
    all_gather x1 -> x0, waiting for transfers between devices: 63.7 us -> none  [sent_together(): lax.all_gather(both, axis, axis=dim, tiled=True)]
    all_to_all x3 -> x0, starting transfers between devices: 34.9 us -> none  [the longest x1 26 us: sent_together_2(): lax.all_to_all(both, axis, split_axis=split_dim, concat_axis=concat_dim,...]
    dot_general x7 -> x0, matrix products: 13.3 us -> none  [the longest x1 4.22 us: on_device(): lax.dot_general(hidden_low, grad_blocks, (((0,), (1,)), ((), ())), prefer...]
    dot_general x2 -> x0, local copies, waits for them, and re-layouts: 10.3 us -> none  [the longest x1 5.45 us: on_device(): lax.dot_general(token_blocks, both_grad, (((1,), (0,)), ((), ())), prefer...]
    ppermute x2 -> x0, starting transfers between devices: 5.79 us -> none  [swapped(): return lax.ppermute(block, axis, route)]
  transfers between devices with their start and end apart: 6 -> 0, of which waited for: 4 -> 0; matrix products, arithmetic and copies ran while one was open for 8% -> 0% of each run, Pallas kernels for 0% -> 0%
where the time goes in v1:
time: 113 us; the launch traced here: 112 us
  Pallas kernels  102 us (90%)
  local copies, waits for them, and re-layouts  8.43 us (7%)
    pallas_call x1, Pallas kernels, on_device(): pl.pallas_call(body, out_shape=(shape((block, LANES), BF16), shape((2, bl...  102 us
    unnamed x20, local copies, waits for them, and re-layouts  8.43 us

profile of v1, /device:TPU:1, one launch (start us, length us, event | category | flops | bytes accessed | tf_op | source)
XLA Modules:
  0.0 111.5 jit_solution(4348616378891521196)
XLA Ops:
  0.6 0.0 copy-start.3
  0.6 0.7 copy-done.3
  1.3 0.7 copy.14.mixing
  2.1 102.4 %shard_map.126 = (bf16[128,128]{1,0:T(8,128)(2,1)}, f32[2,128]{1,0:T(2,128)}, bf16[1,2048,128]{2,1,0:T(8,128)(2,1)}, bf16[1,2048,128]{2,1,0:T(8,128)(2,1)}, bf16...) custom-call(bf16[128,128]{1,0:T(8,128)(2,1)} %tokens.1, bf16[128,128]{1,0:T(8,128)(2,1)} %upstream.1, ...), custom_call_target="tpu_custom_call" | custom-call | tf_op jit(solution)/shard_map/pallas_call | solution.py:441
  104.5 0.0 copy-start.4
  104.5 1.4 %copy.22 = bf16[128,128]{1,0:T(8,128)(2,1)} copy(bf16[128,128]{1,0:T(8,128)(2,1)} %get-tuple-element.28) | data formatting | bytes 65536
  105.9 0.0 copy-done.4
  105.9 0.6 copy.23
  106.4 0.0 copy-start.1
  106.5 1.9 %copy.24 = bf16[1,2048,128]{2,1,0:T(8,128)(2,1)} copy(bf16[1,2048,128]{2,1,0:T(8,128)(2,1)} %get-tuple-element.30) | data formatting | bytes 1048576
  108.4 0.0 copy-done.1
  108.4 0.0 copy-start
  108.4 0.8 copy.25
  109.2 0.4 copy-done
  109.6 0.0 copy-start.2
  109.6 0.8 copy.26
  110.4 0.0 copy-done.2
  110.4 0.0 copy-start.5
  110.4 0.6 copy.27
  111.0 0.0 copy-done.5
  111.0 0.5 copy.28
Async XLA Ops:
  0.6 0.7 copy-start.3
  104.5 1.4 %copy-start.4 = (f32[2,128]{1,0:T(2,128)S(1)}, f32[2,128]{1,0:T(2,128)}, u32[]{:S(2)}) copy-start(f32[2,128]{1,0:T(2,128)} %get-tuple-element.15) | copy-start | bytes 3076
  106.4 1.9 %copy-start.1 = (bf16[1,2048,128]{2,1,0:T(8,128)(2,1)S(1)}, bf16[1,2048,128]{2,1,0:T(8,128)(2,1)}, u32[]{:S(2)}) copy-start(bf16[1,2048,128]{2,1,0:T(8,128)(2,1)} %get-tuple-element.31) | copy-start | bytes 1572868
  108.4 1.2 %copy-start = (bf16[1,128,2048]{2,1,0:T(8,128)(2,1)S(1)}, bf16[1,128,2048]{2,1,0:T(8,128)(2,1)}, u32[]{:S(2)}) copy-start(bf16[1,128,2048]{2,1,0:T(8,128)(2,1)} %get-tuple-element.32) | copy-start | bytes 1572868
  109.6 0.8 copy-start.2
  110.4 0.6 copy-start.5

commit v2 on v1

--- a/solution.py
+++ b/solution.py
@@ -22,10 +22,20 @@
 SEND = 24
 BACK = 16
 LANES = 128
+ORDER = (
+    ("A0", "B0", "R2", "R3", "A1", "C0", "B1", "D0", "A2", "C1", "E0", "B2", "D1")
+    + ("A3", "C2", "E1", "B3", "D2", "F0", "C3", "E2", "F1", "D3", "E3", "F2")
+)
+REACH = NZ // 4
+FAR = 2 * REACH + 1
 
 
 def offset_of(place):
     return (place + 1) // 2 if place % 2 else -(place // 2)
+
+
+def relay_of(place):
+    return REACH if place % 2 else -REACH
 
 
 def opposite(place):
@@ -47,25 +57,29 @@
 
 
 def body(
-    tokens,
-    upstream,
-    routing,
-    mixing,
-    mixing_rows,
+    tokens_hbm,
+    upstream_hbm,
+    routing_hbm,
+    mixing_hbm,
     gate_hbm,
     up_hbm,
     down_hbm,
     token_out,
     mixing_out,
-    gate_out,
-    up_out,
-    down_out,
+    gate_full,
+    up_full,
+    down_full,
     norms_out,
     down_norms_out,
+    tokens,
+    upstream,
+    routing,
+    mixing_rows,
     w_in,
     w_down,
     z_send,
     z_recv,
+    z_relay,
     x_all,
     y_all,
     grads,
@@ -80,15 +94,13 @@
     score_recv,
     back_send,
     back_recv,
-    gate_full,
-    up_full,
-    down_full,
     norms,
     norms_recv,
+    sem_in,
     sem_w,
-    sem_out,
     sem_send,
     sem_z,
+    sem_relay,
     sem_first,
     sem_second,
     sem_core,
@@ -126,6 +138,19 @@
     def await_bytes(ref, sem):
         pltpu.make_async_copy(ref, ref, sem).wait()
 
+    inputs = [
+        pltpu.make_async_copy(source, target, sem_in.at[n])
+        for n, (source, target) in enumerate(
+            (
+                (routing_hbm, routing),
+                (mixing_hbm, mixing_rows),
+                (tokens_hbm, tokens),
+                (upstream_hbm, upstream),
+            )
+        )
+    ]
+    for copy in inputs:
+        copy.start()
     weights = [
         pltpu.make_async_copy(gate_hbm.at[0], w_in.at[:, pl.ds(0, LANES)], sem_w.at[0]),
         pltpu.make_async_copy(up_hbm.at[0], w_in.at[:, pl.ds(LANES, LANES)], sem_w.at[1]),
@@ -135,11 +160,16 @@
         copy.start()
 
     barrier = pltpu.get_barrier_semaphore()
-    for offset in range(1, NZ):
-        pl.semaphore_signal(barrier, inc=1, device_id=at_z(offset), device_id_type=MESH)
+    for place in range(1, FAR):
+        pl.semaphore_signal(
+            barrier, inc=1, device_id=at_z(offset_of(place)), device_id_type=MESH
+        )
     for dy, dx in plane:
         pl.semaphore_signal(barrier, inc=1, device_id=at_plane(dy, dx), device_id_type=MESH)
     pl.semaphore_signal(barrier, inc=1, device_id=partner, device_id_type=MESH)
+
+    for copy in inputs:
+        copy.wait()
 
     block = tokens.shape[0]
     upper = (iota((block, block), 0) < iota((block, block), 1)).astype(BF16)
@@ -168,15 +198,24 @@
     placed = dot((token_hot[0] | token_hot[1]).astype(BF16), tokens[...], ((1,), (0,)))
     cotangent = upstream[...].astype(F32)
     for k in range(2):
-        scaled = (mixing[:, k : k + 1] * cotangent).astype(BF16)
+        factor = jnp.transpose(jnp.broadcast_to(mixing_rows[k : k + 1, :], (LANES, block)))
+        scaled = (factor * cotangent).astype(BF16)
         placed = placed + dot(grad_hot[k], scaled, ((1,), (0,)))
     z_send[...] = placed.reshape(NZ * SEND // 8, 8, LANES).astype(BF16)
     tiles = SEND // 8
     z_recv[0:tiles] = z_send[0:tiles]
 
-    pl.semaphore_wait(barrier, NZ - 1 + len(plane) + 1)
-
-    for place in range(1, NZ):
+    pl.semaphore_wait(barrier, FAR - 1 + len(plane) + 1)
+
+    for place in range(FAR, NZ):
+        send(
+            z_send.at[pl.ds(place * tiles, tiles)],
+            z_relay.at[pl.ds((place - FAR) * tiles, tiles)],
+            0,
+            sem_relay.at[place // GROUP - NQ // 2],
+            at_z(relay_of(place)),
+        )
+    for place in range(1, FAR):
         send(
             z_send.at[pl.ds(place * tiles, tiles)],
             z_recv.at[pl.ds(opposite(place) * tiles, tiles)],
@@ -206,6 +245,22 @@
 
     def other_rows(q):
         return pl.ds(pl.multiple_of(q * ROWS + (1 - core) * HALF, 16), HALF)
+
+    def stage_relay(q):
+        first = max(q * GROUP, FAR)
+        last = (q + 1) * GROUP
+        await_bytes(
+            z_relay.at[pl.ds((first - FAR) * tiles, (last - first) * tiles)],
+            sem_relay.at[q - NQ // 2],
+        )
+        for place in range(first, last):
+            send(
+                z_relay.at[pl.ds((place - FAR) * tiles, tiles)],
+                z_recv.at[pl.ds(opposite(place) * tiles, tiles)],
+                10,
+                sem_z.at[opposite(place) // GROUP],
+                at_z(offset_of(place) - relay_of(place)),
+            )
 
     def stage_gather_first(q):
         count = GROUP * tiles
@@ -333,13 +388,13 @@
                     at_z(offset_of(place)),
                 )
 
-    def weight_in():
+    def weight_in(begin, end):
         def step(b, _):
             x_rows = x_all[b // NX, b % NX]
             full = dot(x_rows, grads[...], ((0,), (0,)))
             at = pl.ds(pl.multiple_of(b * LANES, LANES), LANES)
-            gate_full[at, :] = full[:, :LANES].astype(BF16)
-            up_full[at, :] = full[:, LANES:].astype(BF16)
+            gate_full[0, at, :] = full[:, :LANES].astype(BF16)
+            up_full[0, at, :] = full[:, LANES:].astype(BF16)
             for h in range(2):
                 piece = full[:, h * LANES : (h + 1) * LANES]
                 norms[h : h + 1, at] = jnp.sum(
@@ -347,11 +402,10 @@
                 )
             return 0
 
-        lax.fori_loop(0, NT, step, 0)
-        pltpu.make_async_copy(gate_full, gate_out.at[0], sem_out.at[0]).start()
-        pltpu.make_async_copy(up_full, up_out.at[0], sem_out.at[1]).start()
-        for n, (dy, dx) in enumerate(plane):
-            send(norms, norms_recv.at[n], 9, sem_norm, at_plane(dy, dx))
+        lax.fori_loop(begin, end, step, 0)
+        if end == NT:
+            for n, (dy, dx) in enumerate(plane):
+                send(norms, norms_recv.at[n], 9, sem_norm, at_plane(dy, dx))
 
     def weight_down():
         hidden_t = jnp.transpose(hidden_all[...].astype(F32)).astype(BF16)
@@ -362,29 +416,28 @@
             )
             full = dot(hidden_t, y_rows, ((1,), (0,)))
             at = pl.ds(pl.multiple_of(b * 2 * LANES, 2 * LANES), 2 * LANES)
-            down_full[:, at] = full.astype(BF16)
+            down_full[0, :, at] = full.astype(BF16)
             left, right = full[:, :LANES], full[:, LANES:]
             return squares + left * left + right * right
 
         squares = lax.fori_loop(0, NT // 2, step, jnp.zeros((LANES, LANES), F32))
         down_norms_out[...] = jnp.sum(jnp.transpose(squares), axis=0, keepdims=True)
-        pltpu.make_async_copy(down_full, down_out.at[0], sem_out.at[2]).start()
-
-    stages = (
-        (5, stage_back),
-        (4, stage_pair_sum),
-        (0, stage_gather_first),
-        (1, stage_gather_second),
-        (3, stage_compute),
-        (2, stage_cores),
+
+    stages = dict(
+        A=stage_gather_first,
+        B=stage_gather_second,
+        C=stage_cores,
+        D=stage_compute,
+        E=stage_pair_sum,
+        F=stage_back,
+        R=stage_relay,
     )
-    for step in range(NQ + 5):
-        if step == NQ + 4:
-            weight_in()
-        for depth, stage in stages:
-            if 0 <= step - depth < NQ:
-                stage(step - depth)
+    for name, q in ORDER:
+        stages[name](int(q))
     weight_down()
+    weight_in(0, NT // 2)
+    stage_back(NQ - 1)
+    weight_in(NT // 2, NT)
 
     await_bytes(back_recv.at[pl.ds(BACK, (NZ - 1) * BACK), :], sem_back)
     rows_back = iota((NZ * BACK, block), 0)
@@ -414,8 +467,6 @@
         total = total + norms_recv[n]
     norms_out[0] = total
 
-    for full, out, n in ((gate_full, gate_out, 0), (up_full, up_out, 1), (down_full, down_out, 2)):
-        pltpu.make_async_copy(full, out.at[0], sem_out.at[n]).wait()
     sent = (
         z_recv.at[pl.ds(tiles, (NZ - 1) * tiles)],
         x_all.at[0, pl.ds(0, 3)],
@@ -427,35 +478,54 @@
         score_recv,
         back_recv.at[pl.ds(BACK, (NZ - 1) * BACK), :],
         norms_recv,
+        z_relay,
     )
     for n, ref in enumerate(sent):
         await_bytes(ref, sem_send.at[n])
 
 
+def write_out(*refs):
+    count = len(refs) // 2
+    sems = refs[-1]
+    copies = [
+        pltpu.make_async_copy(refs[n], refs[count + n], sems.at[n]) for n in range(count)
+    ]
+    for copy in copies:
+        copy.start()
+    for copy in copies:
+        copy.wait()
+
+
 def on_device(tokens, routing, mixing, gate_matrix, up_matrix, down_matrix, upstream):
     vmem = pl.BlockSpec(memory_space=pltpu.VMEM)
-    hbm = pl.BlockSpec(memory_space=pl.ANY)
+    hbm = pl.BlockSpec(memory_space=pltpu.HBM)
     block = tokens.shape[0]
     shape = jax.ShapeDtypeStruct
     dma = pltpu.SemaphoreType.DMA
+    shapes = (
+        shape((block, LANES), BF16),
+        shape((2, block), F32),
+        shape(gate_matrix.shape, BF16),
+        shape(up_matrix.shape, BF16),
+        shape(down_matrix.shape, BF16),
+        shape((1, 2, NT * LANES), F32),
+        shape((1, LANES), F32),
+    )
     results = pl.pallas_call(
         body,
-        out_shape=(
-            shape((block, LANES), BF16),
-            shape((2, block), F32),
-            shape(gate_matrix.shape, BF16),
-            shape(up_matrix.shape, BF16),
-            shape(down_matrix.shape, BF16),
-            shape((1, 2, NT * LANES), F32),
-            shape((1, LANES), F32),
-        ),
-        in_specs=[vmem] * 5 + [hbm] * 3,
-        out_specs=(vmem, vmem, hbm, hbm, hbm, vmem, vmem),
+        out_shape=tuple(pltpu.VMEM(s.shape, s.dtype) for s in shapes),
+        in_specs=[hbm] * 7,
+        out_specs=[vmem] * 7,
         scratch_shapes=[
+            pltpu.VMEM((block, LANES), BF16),
+            pltpu.VMEM((block, LANES), BF16),
+            pltpu.VMEM((2, block), jnp.int32),
+            pltpu.VMEM((2, block), F32),
             pltpu.VMEM((NT * LANES, 2 * LANES), BF16),
             pltpu.VMEM((LANES, NT * LANES), BF16),
             pltpu.VMEM((NZ * SEND // 8, 8, LANES), BF16),
             pltpu.VMEM((NZ * SEND // 8, 8, LANES), BF16),
+            pltpu.VMEM(((NZ - FAR) * SEND // 8, 8, LANES), BF16),
             pltpu.VMEM((NY, NX, ALL, LANES), BF16),
             pltpu.VMEM((NY, NX, ALL, LANES), BF16),
             pltpu.VMEM((ALL, 2 * LANES), BF16),
@@ -470,15 +540,13 @@
             pltpu.VMEM((NQ, NT - 1, 1, LANES), F32),
             pltpu.VMEM((NZ * BACK, LANES), BF16),
             pltpu.VMEM((NZ * BACK, LANES), BF16),
-            pltpu.VMEM((NT * LANES, LANES), BF16),
-            pltpu.VMEM((NT * LANES, LANES), BF16),
-            pltpu.VMEM((LANES, NT * LANES), BF16),
             pltpu.VMEM((2, NT * LANES), F32),
             pltpu.VMEM((NT - 1, 2, NT * LANES), F32),
+            dma((4,)),
             dma((3,)),
-            dma((3,)),
-            dma((10,)),
+            dma((11,)),
             dma((NQ,)),
+            dma((NQ // 2,)),
             dma((NQ, 2, 3)),
             dma((NQ, 2, 3)),
             dma((NQ, 2)),
@@ -496,12 +564,18 @@
         tokens,
         upstream,
         routing.T,
-        mixing,
         mixing.T,
         gate_matrix,
         up_matrix,
         down_matrix,
     )
+    results = pl.pallas_call(
+        write_out,
+        out_shape=shapes,
+        in_specs=[vmem] * 7,
+        out_specs=[hbm] * 7,
+        scratch_shapes=[dma((7,))],
+    )(*(pltpu.with_memory_space_constraint(r, pltpu.VMEM) for r in results))
     token_gradient, mixing_t, gate, up, down, norms, down_norms = results
     return token_gradient, mixing_t.T, gate, up, down, norms, down_norms
 

time: 113 us -> 99.4 us (0.88)
  local copies, waits for them, and re-layouts: 8.43 us -> 0 us
  Pallas kernels: 102 us -> 98.2 us
    unnamed x20 -> x0, local copies, waits for them, and re-layouts: 8.43 us -> none
    pallas_call x1 -> x2, Pallas kernels: 102 us -> 98.2 us  [the longest x1 97 us: on_device(): pl.pallas_call(body, out_shape=tuple((pltpu.VMEM(s.shape, s.dtype) for s...]
where the time goes in v2:
time: 99.4 us; the launch traced here: 98.8 us
  Pallas kernels  98.2 us (99%)
    pallas_call x1, Pallas kernels, on_device(): pl.pallas_call(body, out_shape=tuple((pltpu.VMEM(s.shape, s.dtype) for s...  97 us

profile of v2, /device:TPU:1, one launch (start us, length us, event | category | flops | bytes accessed | tf_op | source)
XLA Modules:
  0.0 98.8 jit_solution(16932220842274154173)
XLA Ops:
  0.6 97.0 %shard_map.126 = (bf16[128,128]{1,0:T(8,128)(2,1)S(1)}, f32[2,128]{1,0:T(2,128)S(1)}, bf16[1,2048,128]{2,1,0:T(8,128)(2,1)S(1)}, bf16[1,2048,128]{2,1,0:T(8,128)...) custom-call(bf16[128,128]{1,0:T(8,128)(2,1)} %tokens_hbm.1, ...), custom_call_target="tpu_custom_call" | custom-call | tf_op jit(solution)/shard_map/pallas_call | solution.py:514
  97.6 1.2 %shard_map.127 = (bf16[128,128]{1,0:T(8,128)(2,1)}, f32[2,128]{1,0:T(2,128)}, bf16[1,2048,128]{2,1,0:T(8,128)(2,1)}, bf16[1,2048,128]{2,1,0:T(8,128)(2,1)}, bf16...) custom-call(bf16[128,128]{1,0:T(8,128)(2,1)S(1)} %get-tuple-element.21.refs_0_, ...), custom_call_target="tpu_custom_call" | custom-call | tf_op jit(solution)/shard_map/pallas_call | solution.py:572

commit v3 on v2

--- a/solution.py
+++ b/solution.py
@@ -23,9 +23,10 @@
 BACK = 16
 LANES = 128
 ORDER = (
-    ("A0", "B0", "R2", "R3", "A1", "C0", "B1", "D0", "A2", "C1", "E0", "B2", "D1")
-    + ("A3", "C2", "E1", "B3", "D2", "F0", "C3", "E2", "F1", "D3", "E3", "F2")
+    ("A0", "B0", "R2", "R3", "G0", "A1", "C0", "A2", "A3", "B1", "D0", "B2", "E0", "B3", "G1")
+    + ("G2", "C1", "G3", "C2", "C3", "D1", "H0", "D2", "E1", "F0", "D3", "E2", "E3", "H1")
 )
+SPLIT = 48
 REACH = NZ // 4
 FAR = 2 * REACH + 1
 
@@ -87,7 +88,12 @@
     part,
     part_in,
     part_sum,
-    part_recv,
+    row_recv,
+    col_recv,
+    row_sum,
+    col_sum,
+    row_last,
+    col_last,
     score_own,
     score_in,
     score_sum,
@@ -103,10 +109,14 @@
     sem_relay,
     sem_first,
     sem_second,
+    sem_forward,
     sem_core,
     sem_part,
     sem_score,
-    sem_sum,
+    sem_row,
+    sem_col,
+    sem_row_last,
+    sem_col_last,
     sem_sum_score,
     sem_back,
     sem_norm,
@@ -207,6 +217,14 @@
 
     pl.semaphore_wait(barrier, FAR - 1 + len(plane) + 1)
 
+    for place in range(1, GROUP + 1):
+        send(
+            z_send.at[pl.ds(place * tiles, tiles)],
+            z_recv.at[pl.ds(opposite(place) * tiles, tiles)],
+            0,
+            sem_z.at[opposite(place) // GROUP],
+            at_z(offset_of(place)),
+        )
     for place in range(FAR, NZ):
         send(
             z_send.at[pl.ds(place * tiles, tiles)],
@@ -215,7 +233,7 @@
             sem_relay.at[place // GROUP - NQ // 2],
             at_z(relay_of(place)),
         )
-    for place in range(1, FAR):
+    for place in range(GROUP + 1, FAR):
         send(
             z_send.at[pl.ds(place * tiles, tiles)],
             z_recv.at[pl.ds(opposite(place) * tiles, tiles)],
@@ -282,22 +300,32 @@
     def stage_gather_second(q):
         for d in range(1, NX):
             await_bytes(x_all.at[y, x, own_rows(q), :], sem_first.at[q, 0, d - 1])
-        for d in range(1, NY):
+        for d in (1, NY - 1):
             mine = x_all.at[y, :, own_rows(q), :]
-            send(mine, mine, 2, sem_second.at[q, 0, d - 1], at_plane(d, 0))
+            send(mine, mine, 2, sem_second.at[q, 0, d // 2], at_plane(d, 0))
         for d in range(1, NY):
             await_bytes(y_all.at[y, x, own_rows(q), :], sem_first.at[q, 1, d - 1])
-        for d in range(1, NX):
+        for d in (1, NX - 1):
             mine = y_all.at[:, x, own_rows(q), :]
-            send(mine, mine, 2, sem_second.at[q, 1, d - 1], at_plane(0, d))
+            send(mine, mine, 2, sem_second.at[q, 1, d // 2], at_plane(0, d))
+
+    def stage_forward(q):
+        for n, d in enumerate((1, NY - 1)):
+            await_bytes(x_all.at[y, :, own_rows(q), :], sem_second.at[q, 0, n])
+            theirs = x_all.at[lax.rem(y + NY - d, NY), pl.ds(2 * n, 2), own_rows(q), :]
+            send(theirs, theirs, 11, sem_forward.at[q, 0, n], at_plane(d, 0))
+        for n, d in enumerate((1, NX - 1)):
+            await_bytes(y_all.at[:, x, own_rows(q), :], sem_second.at[q, 1, n])
+            theirs = y_all.at[pl.ds(2 * n, 2), lax.rem(x + NX - d, NX), own_rows(q), :]
+            send(theirs, theirs, 11, sem_forward.at[q, 1, n], at_plane(0, d))
 
     def stage_cores(q):
-        for d in range(1, NY):
-            await_bytes(x_all.at[y, :, own_rows(q), :], sem_second.at[q, 0, d - 1])
+        for n in range(2):
+            await_bytes(x_all.at[y, pl.ds(0, 2), own_rows(q), :], sem_forward.at[q, 0, n])
         mine = x_all.at[:, :, own_rows(q), :]
         send(mine, mine, 3, sem_core.at[q, 0], partner)
-        for d in range(1, NX):
-            await_bytes(y_all.at[:, x, own_rows(q), :], sem_second.at[q, 1, d - 1])
+        for n in range(2):
+            await_bytes(y_all.at[pl.ds(0, 2), x, own_rows(q), :], sem_forward.at[q, 1, n])
         mine = y_all.at[:, :, own_rows(q), :]
         send(mine, mine, 3, sem_core.at[q, 1], partner)
 
@@ -349,23 +377,66 @@
         total = part[:, :, own_rows(q), :].astype(F32) + part_in[q].astype(F32)
         part_sum[q] = total.astype(BF16)
         score_sum[q] = score_own[q, core] + score_in[q]
+        for d in range(1, NX):
+            send(
+                part_sum.at[q, :, lax.rem(x + d, NX), pl.ds(0, SPLIT), :],
+                row_recv.at[q, d - 1],
+                6,
+                sem_row.at[q],
+                at_plane(0, d),
+            )
+        for d in range(1, NY):
+            send(
+                part_sum.at[q, lax.rem(y + d, NY), :, pl.ds(SPLIT, HALF - SPLIT), :],
+                col_recv.at[q, d - 1],
+                12,
+                sem_col.at[q],
+                at_plane(d, 0),
+            )
         for n, (dy, dx) in enumerate(plane):
+            send(score_sum.at[q], score_recv.at[q, n], 7, sem_sum_score.at[q], at_plane(dy, dx))
+
+    def stage_reduce(q):
+        await_bytes(row_recv.at[q], sem_row.at[q])
+        total = part_sum[q, :, x, pl.ds(0, SPLIT), :].astype(F32)
+        for n in range(NX - 1):
+            total = total + row_recv[q, n].astype(F32)
+        row_sum[q] = total.astype(BF16)
+        for d in range(1, NY):
             send(
-                part_sum.at[q, lax.rem(y + dy, NY), lax.rem(x + dx, NX)],
-                part_recv.at[q, n],
-                6,
-                sem_sum.at[q],
-                at_plane(dy, dx),
-            )
-            send(score_sum.at[q], score_recv.at[q, n], 7, sem_sum_score.at[q], at_plane(dy, dx))
+                row_sum.at[q, lax.rem(y + d, NY)],
+                row_last.at[q, d - 1],
+                13,
+                sem_row_last.at[q],
+                at_plane(d, 0),
+            )
+        await_bytes(col_recv.at[q], sem_col.at[q])
+        total = part_sum[q, y, :, pl.ds(SPLIT, HALF - SPLIT), :].astype(F32)
+        for n in range(NY - 1):
+            total = total + col_recv[q, n].astype(F32)
+        col_sum[q] = total.astype(BF16)
+        for d in range(1, NX):
+            send(
+                col_sum.at[q, lax.rem(x + d, NX)],
+                col_last.at[q, d - 1],
+                14,
+                sem_col_last.at[q],
+                at_plane(0, d),
+            )
 
     def stage_back(q):
-        await_bytes(part_recv.at[q], sem_sum.at[q])
+        await_bytes(row_last.at[q], sem_row_last.at[q])
+        await_bytes(col_last.at[q], sem_col_last.at[q])
         await_bytes(score_recv.at[q], sem_sum_score.at[q])
-        total = part_sum[q, y, x].astype(F32)
+        rows = row_sum[q, y].astype(F32)
+        for n in range(NY - 1):
+            rows = rows + row_last[q, n].astype(F32)
+        cols = col_sum[q, x].astype(F32)
+        for n in range(NX - 1):
+            cols = cols + col_last[q, n].astype(F32)
+        total = jnp.concatenate([rows, cols], axis=0)
         score = score_sum[q]
         for n in range(len(plane)):
-            total = total + part_recv[q, n].astype(F32)
             score = score + score_recv[q, n]
         high = score.astype(BF16)
         rest = score - high.astype(F32)
@@ -426,18 +497,25 @@
     stages = dict(
         A=stage_gather_first,
         B=stage_gather_second,
+        G=stage_forward,
         C=stage_cores,
         D=stage_compute,
         E=stage_pair_sum,
+        H=stage_reduce,
         F=stage_back,
         R=stage_relay,
     )
     for name, q in ORDER:
         stages[name](int(q))
     weight_down()
-    weight_in(0, NT // 2)
+    stage_reduce(NQ - 2)
+    stage_back(NQ - 3)
+    weight_in(0, NT // 4)
+    stage_reduce(NQ - 1)
+    stage_back(NQ - 2)
+    weight_in(NT // 4, 5 * NT // 8)
     stage_back(NQ - 1)
-    weight_in(NT // 2, NT)
+    weight_in(5 * NT // 8, NT)
 
     await_bytes(back_recv.at[pl.ds(BACK, (NZ - 1) * BACK), :], sem_back)
     rows_back = iota((NZ * BACK, block), 0)
@@ -470,15 +548,19 @@
     sent = (
         z_recv.at[pl.ds(tiles, (NZ - 1) * tiles)],
         x_all.at[0, pl.ds(0, 3)],
-        x_all.at[pl.ds(0, 3)],
+        x_all.at[pl.ds(0, 2)],
         x_all,
         x_all.at[pl.ds(0, 2)],
         score_in,
-        part_recv,
+        row_recv,
         score_recv,
         back_recv.at[pl.ds(BACK, (NZ - 1) * BACK), :],
         norms_recv,
         z_relay,
+        x_all.at[0],
+        col_recv,
+        row_last,
+        col_last,
     )
     for n, ref in enumerate(sent):
         await_bytes(ref, sem_send.at[n])
@@ -533,7 +615,12 @@
             pltpu.VMEM((NY, NX, ALL, LANES), BF16),
             pltpu.VMEM((NQ, NY, NX, HALF, LANES), BF16),
             pltpu.VMEM((NQ, NY, NX, HALF, LANES), BF16),
-            pltpu.VMEM((NQ, NT - 1, HALF, LANES), BF16),
+            pltpu.VMEM((NQ, NX - 1, NY, SPLIT, LANES), BF16),
+            pltpu.VMEM((NQ, NY - 1, NX, HALF - SPLIT, LANES), BF16),
+            pltpu.VMEM((NQ, NY, SPLIT, LANES), BF16),
+            pltpu.VMEM((NQ, NX, HALF - SPLIT, LANES), BF16),
+            pltpu.VMEM((NQ, NY - 1, SPLIT, LANES), BF16),
+            pltpu.VMEM((NQ, NX - 1, HALF - SPLIT, LANES), BF16),
             pltpu.VMEM((NQ, 2, 1, LANES), F32),
             pltpu.VMEM((NQ, 1, LANES), F32),
             pltpu.VMEM((NQ, 1, LANES), F32),
@@ -544,12 +631,16 @@
             pltpu.VMEM((NT - 1, 2, NT * LANES), F32),
             dma((4,)),
             dma((3,)),
-            dma((11,)),
+            dma((15,)),
             dma((NQ,)),
             dma((NQ // 2,)),
             dma((NQ, 2, 3)),
-            dma((NQ, 2, 3)),
+            dma((NQ, 2, 2)),
+            dma((NQ, 2, 2)),
             dma((NQ, 2)),
+            dma((NQ,)),
+            dma((NQ,)),
+            dma((NQ,)),
             dma((NQ,)),
             dma((NQ,)),
             dma((NQ,)),

time: 99.4 us -> 101 us (1.016)
  Pallas kernels: 98.2 us -> 100 us
    pallas_call x1, Pallas kernels: 97 us -> 98.9 us  [on_device(): pl.pallas_call(body, out_shape=tuple((pltpu.VMEM(s.shape, s.dtype) for s...]
where the time goes in v3:
time: 101 us
  Pallas kernels  100 us (99%)
    pallas_call x1, Pallas kernels, on_device(): pl.pallas_call(body, out_shape=tuple((pltpu.VMEM(s.shape, s.dtype) for s...  98.9 us

profile of v3, /device:TPU:1, one launch (start us, length us, event | category | flops | bytes accessed | tf_op | source)
XLA Modules:
  0.0 100.8 jit_solution(5824247500457881150)
XLA Ops:
  0.6 98.9 %shard_map.126 = (bf16[128,128]{1,0:T(8,128)(2,1)S(1)}, f32[2,128]{1,0:T(2,128)S(1)}, bf16[1,2048,128]{2,1,0:T(8,128)(2,1)S(1)}, bf16[1,2048,128]{2,1,0:T(8,128)...) custom-call(bf16[128,128]{1,0:T(8,128)(2,1)} %tokens_hbm.1, ...), custom_call_target="tpu_custom_call" | custom-call | tf_op jit(solution)/shard_map/pallas_call | solution.py:596
  99.6 1.2 %shard_map.127 = (bf16[128,128]{1,0:T(8,128)(2,1)}, f32[2,128]{1,0:T(2,128)}, bf16[1,2048,128]{2,1,0:T(8,128)(2,1)}, bf16[1,2048,128]{2,1,0:T(8,128)(2,1)}, bf16...) custom-call(bf16[128,128]{1,0:T(8,128)(2,1)S(1)} %get-tuple-element.21.refs_0_, ...), custom_call_target="tpu_custom_call" | custom-call | tf_op jit(solution)/shard_map/pallas_call | solution.py:663
